TPU v7x, 32 devices: a whole 2x2x4 slice. The times are simulated.
32 devices in a mesh: ep: 16 (over z, y, x), tp: 2 (over core).
Axes of the slice: x: 2, y: 2, z: 4, core: 2. Of those that a mesh axis runs over, the one named last changes fastest.
Arguments:
- tokens: bfloat16 [768, 2048], P('ep', 'tp'), may hold values from -12 to 12
- conv_state: bfloat16 [768, 3, 1024], P('ep', None, 'tp'), may hold values from -6 to 6
- hidden_state: float32 [768, 1024], P('ep', 'tp'), may hold values from -6 to 6
- mixer_gain: float32 [2048], replicated, may hold values from 0.1 to 1.9
- branch_weight: bfloat16 [2048, 1024], P(None, 'tp'), may hold values from -0.125 to 0.125
- gelu_weight: bfloat16 [2048, 1024], P(None, 'tp'), may hold values from -0.125 to 0.125
- conv_kernel: float32 [4, 1024], P(None, 'tp'), may hold values from -3 to 3
- recur_blocks: bfloat16 [16, 64, 64], P('tp'), may hold values from -0.75 to 0.75
- input_blocks: bfloat16 [16, 64, 64], P('tp'), may hold values from -0.75 to 0.75
- decay_rate: float32 [1024], P('tp'), may hold values from 0.002 to 0.1
- output_weight: bfloat16 [1024, 2048], P(None, 'tp'), may hold values from -0.1875 to 0.1875
- expert_gain: float32 [2048], replicated, may hold values from 0.1 to 1.9
- expert_ids: int32 [768, 2], P('ep'), may hold values from 0 to 15, as said below
- group_prob: float32 [768], P('ep'), may hold values from 0.25 to 1
- expert_logit: float32 [768, 2], P('ep'), may hold values from -4 to 4
- expert_gate: bfloat16 [16, 2048, 512], P('ep', None, 'tp'), may hold values from -0.125 to 0.125
- expert_up: bfloat16 [16, 2048, 512], P('ep', None, 'tp'), may hold values from -0.125 to 0.125
- expert_down: bfloat16 [16, 512, 2048], P('ep', 'tp'), may hold values from -0.25 to 0.25
Outputs:
- layer_out: bfloat16 [768, 2048], P('ep', 'tp')
- new_hidden: float32 [768, 1024], P('ep', 'tp')
Inputs may be any that keep to these rules, and one draw needn't show every extreme that they name: `expert_ids`: the two experts of a row are different and lie in one group of 4 consecutive experts. Within the rows of one index of ep no expert is named more than 6 times, and one expert is named exactly 6 times by the rows of every index of ep.
All inputs are finite; a program needn't handle non-finite values.
Results may differ from a plain program's by a relative error of at most 0.012.
Values may be sent and summed in bfloat16 or wider, within the bound.
A program may use at most 64 MiB of HBM per device.

v0:
```python
import jax
import jax.numpy as jnp
from jax import lax
from jax.sharding import PartitionSpec as P

EPSILON = 1e-06
RATE_SCALE = 8.0


def normalize(values, gain_row):
    squares = jnp.mean(values * values, axis=-1, keepdims=True)
    return values * lax.rsqrt(squares + EPSILON) * gain_row


def local(
    tokens,
    conv_state,
    hidden_state,
    mixer_gain,
    branch_weight,
    gelu_weight,
    conv_kernel,
    recur_blocks,
    input_blocks,
    decay_rate,
    output_weight,
    expert_gain,
    expert_ids,
    group_prob,
    expert_logit,
    expert_gate,
    expert_up,
    expert_down,
):
    whole_tokens = lax.all_gather(tokens, "tp", axis=1, tiled=True)
    normed = normalize(whole_tokens.astype(jnp.float32), mixer_gain).astype(jnp.bfloat16)
    branch = jnp.dot(normed, branch_weight, preferred_element_type=jnp.float32).astype(jnp.bfloat16)
    gelu_input = jnp.dot(normed, gelu_weight, preferred_element_type=jnp.float32).astype(
        jnp.bfloat16
    )
    window = jnp.concatenate([conv_state, branch[:, None, :]], axis=1).astype(jnp.float32)
    convolved = jnp.sum(window * conv_kernel[None], axis=1).astype(jnp.bfloat16)
    sequences, channels = convolved.shape
    blocks, block_size = (recur_blocks.shape[0], recur_blocks.shape[1])
    grouped = convolved.reshape(sequences, blocks, block_size)
    recur_pre = jnp.einsum(
        "tnc,ncd->tnd", grouped, recur_blocks, preferred_element_type=jnp.float32
    ).reshape(sequences, channels)
    input_pre = jnp.einsum(
        "tnc,ncd->tnd", grouped, input_blocks, preferred_element_type=jnp.float32
    ).reshape(sequences, channels)
    recur_gate = jax.nn.sigmoid(recur_pre)
    input_gate = jax.nn.sigmoid(input_pre)
    log_decay = -RATE_SCALE * recur_gate * decay_rate
    new_hidden = jnp.exp(log_decay) * hidden_state + jnp.sqrt(-jnp.expm1(2.0 * log_decay)) * (
        input_gate * convolved.astype(jnp.float32)
    )
    mixed_rows = (
        new_hidden * jax.nn.gelu(gelu_input.astype(jnp.float32), approximate=True)
    ).astype(jnp.bfloat16)
    mixed_whole = lax.all_gather(mixed_rows, "tp", axis=1, tiled=True)
    residual = (
        tokens.astype(jnp.float32)
        + jnp.dot(mixed_whole, output_weight, preferred_element_type=jnp.float32)
    ).astype(jnp.bfloat16)
    experts = lax.axis_size("ep")
    top_count = expert_ids.shape[1]
    capacity = 2 * max(1, sequences // experts)
    flat_ids = expert_ids.reshape(-1)
    onehot_ids = (flat_ids[:, None] == jnp.arange(experts, dtype=jnp.int32)[None, :]).astype(
        jnp.int32
    )
    earlier = jnp.cumsum(onehot_ids, axis=0) - onehot_ids
    ranking = jnp.sum(earlier * onehot_ids, axis=1)
    slot_index = flat_ids * capacity + ranking
    placing = (
        jnp.arange(experts * capacity, dtype=jnp.int32)[:, None] == slot_index[None, :]
    ).astype(jnp.float32)
    placing = jnp.sum(placing.reshape(experts * capacity, sequences, top_count), axis=2).astype(
        jnp.bfloat16
    )
    values = residual.astype(jnp.float32)
    half_width = values.shape[1]
    square_total = lax.psum(jnp.sum(values * values, axis=1), "tp")
    gain_part = lax.dynamic_slice_in_dim(
        expert_gain, lax.axis_index("tp") * half_width, half_width, 0
    )
    scaling = lax.rsqrt(square_total / (half_width * lax.axis_size("tp")) + EPSILON)
    moe_input = (values * scaling[:, None] * gain_part[None, :]).astype(jnp.bfloat16)
    outgoing = jnp.dot(placing, moe_input, preferred_element_type=jnp.float32).astype(jnp.bfloat16)
    outgoing = outgoing.reshape(experts, capacity, half_width)
    received = lax.all_gather(
        lax.all_to_all(outgoing, "ep", split_axis=0, concat_axis=0, tiled=True),
        "tp",
        axis=2,
        tiled=True,
    )
    sources, slot_count, features = received.shape
    flat_rows = received.reshape(sources * slot_count, features)
    gate_part = jnp.dot(flat_rows, expert_gate[0], preferred_element_type=jnp.float32)
    upper_part = jnp.dot(flat_rows, expert_up[0], preferred_element_type=jnp.float32)
    hidden_units = (jax.nn.silu(gate_part) * upper_part).astype(jnp.bfloat16)
    partial_value = jnp.dot(
        hidden_units, expert_down[0], preferred_element_type=jnp.float32
    ).reshape(sources, slot_count, features)
    summed = lax.psum_scatter(
        partial_value.astype(jnp.bfloat16), "tp", scatter_dimension=2, tiled=True
    )
    returned = lax.all_to_all(summed, "ep", split_axis=0, concat_axis=0, tiled=True)
    out_width = returned.shape[2]
    picked = jnp.take(returned.reshape(experts * capacity, out_width), slot_index, axis=0).reshape(
        sequences, top_count, out_width
    )
    logit_exp = jnp.exp(expert_logit)
    weights = group_prob[:, None] * logit_exp / jnp.sum(logit_exp, axis=1, keepdims=True)
    layer_out = (
        residual.astype(jnp.float32)
        + jnp.sum(weights[:, :, None] * picked.astype(jnp.float32), axis=1)
    ).astype(jnp.bfloat16)
    return (layer_out, new_hidden)


def solution(mesh):
    return jax.shard_map(
        local,
        mesh=mesh,
        in_specs=(
            P("ep", "tp"),
            P("ep", None, "tp"),
            P("ep", "tp"),
            P(),
            P(None, "tp"),
            P(None, "tp"),
            P(None, "tp"),
            P("tp", None, None),
            P("tp", None, None),
            P("tp"),
            P(None, "tp"),
            P(),
            P("ep", None),
            P("ep"),
            P("ep", None),
            P("ep", None, "tp"),
            P("ep", None, "tp"),
            P("ep", "tp", None),
        ),
        out_specs=(P("ep", "tp"), P("ep", "tp")),
        check_vma=False,
    )
```

profile of v0, /device:TPU:0, one launch (start us, length us, event | category | flops | bytes accessed | tf_op | source)
XLA Modules:
  0.0 81.5 jit_solution(5412062372316779908)
XLA Ops:
  7.3 2.4 %all_gather.9 = bf16[48,2048]{1,0:T(8,128)(2,1)S(1)} all-gather(bf16[48,1024]{1,0:T(8,128)(2,1)} %param.18), channel_id=1, replica_groups=mesh['ep'=16,'tp'=2] {'tp'}, dimensions={1}, use_global_device_ids=true | all-gather | bytes 294912 | tf_op jit(solution)/shard_map/all_gather | solution.py:35
  9.7 0.1 fusion.17
  9.8 2.2 %fusion.12 = bf16[48,1,512]{2,0,1:T(8,128)(2,1)S(1)} fusion(bf16[2048,512]{1,0:T(8,128)(2,1)} %param.22, bf16[48,2048]{1,0:T(8,128)(2,1)S(1)} %all_gather.9, f32[2048]{0:T(1024)} %param.21, f32[48]{0:T(128)S(1)} %add_rsqrt_fusion.1), kind=kOutput, calls=%fused_computation.21 | convolution fusion | flops 101081088 | bytes 2351296 | tf_op jit(solution)/shard_map/dot_general | solution.py:37
  12.2 0.2 fusion.7
  12.6 0.2 fusion.3
  13.2 2.2 %fusion.28 = bf16[48,512]{1,0:T(8,128)(2,1)S(1)} fusion(f32[48,512]{1,0:T(8,128)S(1)} %multiply_add_fusion, bf16[2048,512]{1,0:T(8,128)(2,1)} %param.23, bf16[48,2048]{1,0:T(8,128)(2,1)S(1)} %all_gather.9, f32[2048]{0:T(1024)S(1)} %copy-done.5, f32[48]{0:T(128)S(1)} %add_rsqrt_fusion.1), kind=kOutput, calls=%fused_computation.46 | convolution fusion | flops 101351424 | bytes 2449600 | tf_op jit(solution)/shard_map/dot_general | solution.py:38
  15.4 1.9 %all_gather.10 = bf16[48,1024]{1,0:T(8,128)(2,1)S(1)} all-gather(bf16[48,512]{1,0:T(8,128)(2,1)S(1)} %fusion.28), channel_id=1, replica_groups=mesh['ep'=16,'tp'=2] {'tp'}, dimensions={1}, use_global_device_ids=true | all-gather | bytes 147456 | tf_op jit(solution)/shard_map/all_gather | solution.py:61
  17.3 0.6 multiply_reduce_fusion.2
  17.9 2.5 %psum.7 = f32[48]{0:T(128)S(1)} all-reduce(f32[48]{0:T(128)S(1)} %get-tuple-element.4), channel_id=1, replica_groups=mesh['ep'=16,'tp'=2] {'tp'}, use_global_device_ids=true, to_apply=%region_7.8 | all-reduce | flops 48 | bytes 384 | tf_op jit(solution)/shard_map/psum | solution.py:84
  20.7 0.1 reduce_window_sum.11
  20.8 0.2 select_reduce_fusion
  21.3 0.3 convolution_convert_fusion.1
  21.7 18.2 %all_to_all.10 = bf16[16,6,1024]{2,1,0:T(8,128)(2,1)S(1)} all-to-all(bf16[16,6,1024]{2,1,0:T(8,128)(2,1)S(1)} %reshape.112), channel_id=1, replica_groups=mesh['ep'=16,'tp'=2] {'ep'}, dimensions={0} | all-to-all | bytes 393216 | tf_op jit(solution)/shard_map/all_to_all | solution.py:93
  39.9 2.2 %all_gather.11 = bf16[16,6,2048]{2,1,0:T(8,128)(2,1)S(1)} all-gather(bf16[16,6,1024]{2,1,0:T(8,128)(2,1)S(1)} %all_to_all.10), channel_id=1, replica_groups=mesh['ep'=16,'tp'=2] {'tp'}, dimensions={2}, use_global_device_ids=true | all-gather | bytes 589824 | tf_op jit(solution)/shard_map/all_gather | solution.py:92
  42.2 1.5 %fusion.15 = f32[96,256]{1,0:T(8,128)S(1)} fusion(bf16[96,2048]{1,0:T(8,128)(2,1)S(1)} %reshape.113, bf16[1,2048,256]{2,1,0:T(8,128)(2,1)} %param.33), kind=kOutput, calls=%fused_computation.24 | convolution fusion | flops 100663296 | bytes 1540096 | tf_op jit(solution)/shard_map/dot_general | solution.py:100
  43.7 1.5 %fusion.10 = bf16[96,256]{1,0:T(8,128)(2,1)S(1)} fusion(bf16[96,2048]{1,0:T(8,128)(2,1)S(1)} %reshape.113, bf16[1,2048,256]{2,1,0:T(8,128)(2,1)} %param.34, f32[96,256]{1,0:T(8,128)S(1)} %fusion.15), kind=kOutput, calls=%fused_computation.17 | convolution fusion | flops 100810752 | bytes 1589248 | tf_op jit(solution)/shard_map/dot_general | solution.py:101
  45.3 2.3 %convolution_convert_fusion = bf16[16,6,2048]{2,0,1:T(8,128)(2,1)} fusion(bf16[1,256,2048]{2,1,0:T(8,128)(2,1)} %param.35, bf16[16,6,256]{2,1,0:T(8,128)(2,1)S(1)} %dot_general.37), kind=kOutput, calls=%fused_computation.1 | convolution fusion | flops 100859904 | bytes 1490944 | tf_op jit(solution)/shard_map/dot_general | solution.py:103
  47.7 5.8 %reduce-scatter.2.cloned.1.call-done = bf16[16,6,1024]{2,0,1:T(8,128)(2,1)} async-done(((bf16[16,6,2048]{2,0,1:T(8,128)(2,1)}), bf16[16,6,1024]{2,0,1:T(8,128)(2,1)}) %reduce-scatter.2.cloned.1.call-update) | async-done | bytes 196624 | tf_op jit(solution)/shard_map/reduce_scatter | solution.py:106
  53.5 1.7 %copy.63 = bf16[16,6,1024]{2,1,0:T(8,128)(2,1)} copy(bf16[16,6,1024]{2,0,1:T(8,128)(2,1)} %reduce-scatter.2.cloned.1.call-done) | data formatting | bytes 393216 | tf_op jit(solution)/shard_map/reduce_scatter | solution.py:106
  55.2 6.7 %all-to-all-start.1 = ((bf16[16,6,1024]{2,1,0:T(8,128)(2,1)}), bf16[16,6,1024]{2,1,0:T(8,128)(2,1)S(1)}, u32[]{:S(2)}, u32[]{:S(2)}) async-start(bf16[16,6,1024]{2,1,0:T(8,128)(2,1)} %copy.63), calls=%async_computation.2 | async-start | bytes 524288 | tf_op jit(solution)/shard_map/all_to_all | solution.py:109
  62.4 9.9 %all-to-all-done.1 = bf16[16,6,1024]{2,1,0:T(8,128)(2,1)S(1)} async-done(((bf16[16,6,1024]{2,1,0:T(8,128)(2,1)}), bf16[16,6,1024]{2,1,0:T(8,128)(2,1)S(1)}, u32[]{:S(2)}, u32[]{:S(2)}) %all-to-all-start.1) | async-done | bytes 196640 | tf_op jit(solution)/shard_map/all_to_all | solution.py:109
  72.4 0.8 gather_fusion
  73.3 0.7 multiply_reduce_fusion
  74.0 0.7 add_convert_fusion
  (62 shorter events, 2.2 us)
Async XLA Ops:
  7.2 10.1 %copy-start = (bf16[1024,1024]{1,0:T(8,128)(2,1)S(1)}, bf16[1024,1024]{1,0:T(8,128)(2,1)}, u32[]{:S(2)}) copy-start(bf16[1024,1024]{1,0:T(8,128)(2,1)} %param.28) | copy-start | bytes 6291460
  7.2 4.8 %copy-start.3 = (bf16[48,3,512]{2,0,1:T(8,128)(2,1)S(1)}, bf16[48,3,512]{2,0,1:T(8,128)(2,1)}, u32[]{:S(2)}) copy-start(bf16[48,3,512]{2,0,1:T(8,128)(2,1)} %param.19) | copy-start | bytes 442372
  7.2 4.8 %copy-start.7 = (f32[4,512]{1,0:T(4,128)S(1)}, f32[4,512]{1,0:T(4,128)}, u32[]{:S(2)}) copy-start(f32[4,512]{1,0:T(4,128)} %param.24) | copy-start | bytes 24580
  7.2 5.0 %copy-start.12 = (bf16[8,64,64]{2,1,0:T(8,128)(2,1)S(1)}, bf16[8,64,64]{2,1,0:T(8,128)(2,1)}, u32[]{:S(2)}) copy-start(bf16[8,64,64]{2,1,0:T(8,128)(2,1)} %param.25) | copy-start | bytes 196612
  7.2 46.3 %reduce-scatter.2.cloned.1.call-start = ((), (), s32[]{:S(2)}) async-start(), calls=%async_computation.3 | async-start | bytes 589824 | tf_op jit(solution)/shard_map/reduce_scatter | solution.py:106
  9.8 2.8 %copy-start.13 = (bf16[8,64,64]{2,1,0:T(8,128)(2,1)S(1)}, bf16[8,64,64]{2,1,0:T(8,128)(2,1)}, u32[]{:S(2)}) copy-start(bf16[8,64,64]{2,1,0:T(8,128)(2,1)} %param.26) | copy-start | bytes 196612
  12.0 1.0 %copy-start.9 = (f32[512]{0:T(512)S(1)}, f32[512]{0:T(512)}, u32[]{:S(2)}) copy-start(f32[512]{0:T(512)} %param.27) | copy-start | bytes 6148
  12.0 1.0 %copy-start.4 = (f32[48,512]{1,0:T(8,128)S(1)}, f32[48,512]{1,0:T(8,128)}, u32[]{:S(2)}) copy-start(f32[48,512]{1,0:T(8,128)} %param.20) | copy-start | bytes 294916
  12.1 1.1 %copy-start.5 = (f32[2048]{0:T(1024)S(1)}, f32[2048]{0:T(1024)}, u32[]{:S(2)}) copy-start(f32[2048]{0:T(1024)} %param.21) | copy-start | bytes 24580
  12.8 4.4 %copy-start.1 = (bf16[48,1024]{1,0:T(8,128)(2,1)S(1)}, bf16[48,1024]{1,0:T(8,128)(2,1)}, u32[]{:S(2)}) copy-start(bf16[48,1024]{1,0:T(8,128)(2,1)} %param.18) | copy-start | bytes 294916
  13.2 4.7 %copy-start.2 = (f32[48,512]{1,0:T(8,128)}, f32[48,512]{1,0:T(8,128)S(1)}, u32[]{:S(2)}) copy-start(f32[48,512]{1,0:T(8,128)S(1)} %multiply_add_fusion) | copy-start | bytes 294916
  13.2 7.2 %copy-start.6 = (s32[48,2]{0,1:T(2,128)S(1)}, s32[48,2]{0,1:T(2,128)}, u32[]{:S(2)}) copy-start(s32[48,2]{0,1:T(2,128)} %param.30) | copy-start | bytes 1156
  15.4 5.9 %copy-start.8 = (f32[2048]{0:T(1024)S(1)}, f32[2048]{0:T(1024)}, u32[]{:S(2)}) copy-start(f32[2048]{0:T(1024)} %param.29) | copy-start | bytes 24580
  43.7 3.9 %copy-start.10 = (f32[48,2]{0,1:T(2,128)S(1)}, f32[48,2]{0,1:T(2,128)}, u32[]{:S(2)}) copy-start(f32[48,2]{0,1:T(2,128)} %param.32) | copy-start | bytes 1156
  43.7 3.9 %copy-start.11 = (f32[48]{0:T(128)S(1)}, f32[48]{0:T(128)}, u32[]{:S(2)}) copy-start(f32[48]{0:T(128)} %param.31) | copy-start | bytes 580
  55.2 17.1 %all-to-all-start.1 = ((bf16[16,6,1024]{2,1,0:T(8,128)(2,1)}), bf16[16,6,1024]{2,1,0:T(8,128)(2,1)S(1)}, u32[]{:S(2)}, u32[]{:S(2)}) async-start(bf16[16,6,1024]{2,1,0:T(8,128)(2,1)} %copy.63), calls=%async_computation.2 | async-start | bytes 524288 | tf_op jit(solution)/shard_map/all_to_all | solution.py:109
Sparse Core Ops, SparseCore 0:
  47.7 5.7 reduce-scatter.1
where the time goes:
time: 82 us; the launch traced here: 81.5 us
  blocking collectives  27.2 us (33%)
  waiting for transfers between devices  15.8 us (19%)
  between operations  14.4 us (18%)
  matrix products  10.9 us (13%)
  starting transfers between devices  6.77 us (8%)
  local copies, waits for them, and re-layouts  4.27 us (5%)
  other arithmetic  2.18 us (3%)
    all_to_all x1, blocking collectives, local(): lax.all_to_all(outgoing, 'ep', split_axis=0, concat_axis=0, tiled=True)  18.2 us
    all_to_all x1, waiting for transfers between devices, local(): lax.all_to_all(summed, 'ep', split_axis=0, concat_axis=0, tiled=True)  9.95 us
    all_to_all x1, starting transfers between devices, local(): lax.all_to_all(summed, 'ep', split_axis=0, concat_axis=0, tiled=True)  6.73 us
    reduce_scatter x1, waiting for transfers between devices, local(): lax.psum_scatter(partial_value.astype(jnp.bfloat16), 'tp', scatter_dimens...  5.84 us
    psum x1, blocking collectives, local(): square_total = lax.psum(jnp.sum(values * values, axis=1), 'tp')  2.49 us
    all_gather x1, blocking collectives, local(): whole_tokens = lax.all_gather(tokens, 'tp', axis=1, tiled=True)  2.42 us
    dot_general x1, matrix products, local(): jnp.dot(hidden_units, expert_down[0], preferred_element_type=jnp.float32)  2.27 us
    dot_general x1, matrix products, local(): jnp.dot(normed, gelu_weight, preferred_element_type=jnp.float32)  2.18 us
  transfers between devices with their start and end apart: 2, of which 2 were waited for; matrix products, arithmetic and copies ran while one was open for 1% of the time, Pallas kernels for 0%

commit v1 on v0

v1 whole, which is shorter than its diff:
```python
import functools

import jax
import jax.numpy as jnp
from jax import lax
from jax.experimental import pallas as pl
from jax.experimental.pallas import tpu as pltpu
from jax.sharding import PartitionSpec as P

EPSILON = 1e-06
RATE_SCALE = 8.0
MESH = pl.DeviceIdType.MESH
F32 = jnp.float32
BF16 = jnp.bfloat16


def iota(shape, dim):
    return lax.broadcasted_iota(jnp.int32, shape, dim)


def dot(a, b):
    return jnp.dot(a, b, preferred_element_type=F32)


def minus_expm1(z):
    series = 1.0
    for term in (7.0, 6.0, 5.0, 4.0, 3.0, 2.0):
        series = 1.0 + z * (1.0 / term) * series
    return jnp.where(z > -0.35, -z * series, 1.0 - jnp.exp(z))


def kernel(
    n_ep,
    cap,
    tokens,
    conv_state,
    hidden_state,
    mixer_gain,
    branch_weight,
    gelu_weight,
    conv_kernel,
    recur_blocks,
    input_blocks,
    decay_rate,
    output_weight,
    expert_gain,
    expert_ids,
    group_prob,
    expert_logit,
    expert_gate,
    expert_up,
    expert_down,
    layer_out,
    new_hidden_ref,
    w_branch,
    w_gelu,
    w_out,
    w_gate,
    w_up,
    w_down,
    tok,
    mixed,
    squares,
    outgoing,
    recv,
    stage,
    hid,
    ret,
    back,
    back_stage,
    load_sem,
    pair_send,
    pair_recv,
    far_send,
    far_recv,
):
    ep = lax.axis_index("ep")
    tp = lax.axis_index("tp")
    other = 1 - tp
    seq, half = tokens.shape
    chans = hidden_state.shape[1]
    pad = stage.shape[2]
    slots = n_ep * pad

    mine = pl.ds(pl.multiple_of(tp * half, half), half)
    theirs = pl.ds(pl.multiple_of(other * half, half), half)

    loads = [
        pltpu.make_async_copy(branch_weight.at[mine], w_branch.at[tp], load_sem.at[0]),
        pltpu.make_async_copy(gelu_weight.at[mine], w_gelu.at[tp], load_sem.at[1]),
        pltpu.make_async_copy(branch_weight.at[theirs], w_branch.at[other], load_sem.at[2]),
        pltpu.make_async_copy(gelu_weight.at[theirs], w_gelu.at[other], load_sem.at[3]),
        pltpu.make_async_copy(output_weight, w_out, load_sem.at[4]),
        pltpu.make_async_copy(expert_gate.at[0], w_gate, load_sem.at[5]),
        pltpu.make_async_copy(expert_up.at[0], w_up, load_sem.at[6]),
        pltpu.make_async_copy(expert_down.at[0, :, mine], w_down.at[tp], load_sem.at[7]),
    ]
    for load in loads:
        load.start()

    barrier = pltpu.get_barrier_semaphore()
    pl.semaphore_signal(barrier, inc=1, device_id=(ep, other), device_id_type=MESH)

    def greet(step, carry):
        pl.semaphore_signal(
            barrier, inc=1, device_id=(lax.rem(ep + step, n_ep), tp), device_id_type=MESH
        )
        return carry

    lax.fori_loop(1, n_ep, greet, 0)

    def to_pair(src, dst, index):
        return pltpu.make_async_remote_copy(
            src_ref=src,
            dst_ref=dst,
            send_sem=pair_send.at[index],
            recv_sem=pair_recv.at[index],
            device_id=(ep, other),
            device_id_type=MESH,
        )

    stage[...] = jnp.zeros_like(stage)
    back_stage[...] = jnp.zeros_like(back_stage)
    eye = iota((seq, seq), 0) == iota((seq, seq), 1)
    ids = expert_ids[...]
    first, second = ids[:, 0:1], ids[:, 1:2]
    lane_e = iota((seq, n_ep), 1)
    is_first, is_second = lane_e == first, lane_e == second
    named = jnp.where(is_first | is_second, 1.0, 0.0).astype(BF16)
    before = jnp.where(iota((seq, seq), 1) < iota((seq, seq), 0), 1.0, 0.0).astype(BF16)
    earlier = dot(before, named)

    def slot_of(chosen, hits):
        rank = jnp.sum(jnp.where(hits, earlier, 0.0), axis=1, keepdims=True)
        return chosen.astype(F32) * float(pad) + rank

    slot_a, slot_b = slot_of(first, is_first), slot_of(second, is_second)

    def as_row(column):
        return jnp.sum(jnp.where(eye, column, 0.0), axis=0, keepdims=True)

    lane_s = iota((seq, slots), 1).astype(F32)
    pick_a = jnp.where(lane_s == slot_a, 1.0, 0.0).astype(BF16)
    pick_b = jnp.where(lane_s == slot_b, 1.0, 0.0).astype(BF16)
    row_s = iota((slots, seq), 0).astype(F32)
    placed = (row_s == as_row(slot_a)) | (row_s == as_row(slot_b))
    placing = jnp.where(placed, 1.0, 0.0).astype(BF16)
    prob = jnp.sum(jnp.where(eye, group_prob[...], 0.0), axis=1, keepdims=True)
    logit_exp = jnp.exp(expert_logit[...])
    weights = prob * logit_exp / jnp.sum(logit_exp, axis=1, keepdims=True)

    taps = conv_kernel[...]
    stored = jnp.sum(conv_state[...].astype(F32) * taps[None, :3], axis=1)

    blocks, block = recur_blocks.shape[0], recur_blocks.shape[1]
    wide = 2 * block
    twice = jnp.where(
        lax.rem(iota((block, wide), 1), block) == iota((block, wide), 0), 1.0, 0.0
    ).astype(BF16)
    on_diagonal = (iota((wide, wide), 0) < block) == (iota((wide, wide), 1) < block)

    def pair_map(ref, index):
        rows = jnp.concatenate([ref[2 * index], ref[2 * index + 1]], axis=0)
        return jnp.where(on_diagonal, dot(rows, twice), 0.0).astype(BF16)

    recur_maps = [pair_map(recur_blocks, i) for i in range(blocks // 2)]
    input_maps = [pair_map(input_blocks, i) for i in range(blocks // 2)]

    own = tokens[...].astype(F32)
    own_scaled = (own * mixer_gain[:, mine]).astype(BF16)
    own_square = jnp.sum(own * own, axis=1, keepdims=True)
    loads[0].wait()
    branch = dot(own_scaled, w_branch[tp])
    loads[1].wait()
    gelu_input = dot(own_scaled, w_gelu[tp])

    pl.semaphore_wait(barrier, n_ep)
    send_tokens = to_pair(tokens, tok, 0)
    send_tokens.start()
    send_down = to_pair(expert_down.at[0, :, theirs], w_down.at[tp], 1)
    send_down.start()

    send_tokens.wait_recv()
    peer = tok[...].astype(F32)
    peer_scaled = (peer * mixer_gain[:, theirs]).astype(BF16)
    total_square = own_square + jnp.sum(peer * peer, axis=1, keepdims=True)
    scale = lax.rsqrt(total_square / (2 * half) + EPSILON)
    loads[2].wait()
    branch = ((branch + dot(peer_scaled, w_branch[other])) * scale).astype(BF16)
    loads[3].wait()
    gelu_input = ((gelu_input + dot(peer_scaled, w_gelu[other])) * scale).astype(BF16)

    convolved = (stored + branch.astype(F32) * taps[3:4]).astype(BF16)
    pieces = [convolved[:, wide * i : wide * (i + 1)] for i in range(blocks // 2)]
    recur_pre = jnp.concatenate([dot(x, m) for x, m in zip(pieces, recur_maps)], axis=1)
    input_pre = jnp.concatenate([dot(x, m) for x, m in zip(pieces, input_maps)], axis=1)
    recur_gate = jax.nn.sigmoid(recur_pre)
    input_gate = jax.nn.sigmoid(input_pre)
    log_decay = -RATE_SCALE * recur_gate * decay_rate[...]
    new_hidden = jnp.exp(log_decay) * hidden_state[...] + jnp.sqrt(
        minus_expm1(2.0 * log_decay)
    ) * (input_gate * convolved.astype(F32))
    mixed[tp] = (new_hidden * jax.nn.gelu(gelu_input.astype(F32), approximate=True)).astype(BF16)
    send_mixed = to_pair(mixed.at[tp], mixed.at[tp], 2)
    send_mixed.start()
    new_hidden_ref[...] = new_hidden
    loads[4].wait()
    my_rows = pl.ds(pl.multiple_of(tp * chans, chans), chans)
    their_rows = pl.ds(pl.multiple_of(other * chans, chans), chans)
    residual = own + dot(mixed[tp], w_out[my_rows])
    send_mixed.wait_recv()
    residual = (residual + dot(mixed[other], w_out[their_rows])).astype(BF16)

    values = residual.astype(F32)
    mine_square = jnp.sum(values * values, axis=1, keepdims=True)
    squares[tp] = jnp.broadcast_to(mine_square, squares.shape[1:])
    send_squares = to_pair(squares.at[tp], squares.at[tp], 3)
    send_squares.start()
    chosen = dot(placing, residual) * expert_gain[:, mine]
    send_squares.wait_recv()
    both = mine_square + squares[other][:, 0:1]
    scaling = as_row(lax.rsqrt(both / (2 * half) + EPSILON))
    slot_scale = jnp.sum(jnp.where(placed, scaling, 0.0), axis=1, keepdims=True)
    chosen = (chosen * slot_scale).reshape(n_ep, pad, half)
    outgoing[...] = chosen[:, :cap].astype(BF16)

    def far(src, dst, to, index):
        return pltpu.make_async_remote_copy(
            src_ref=src,
            dst_ref=dst,
            send_sem=far_send.at[index],
            recv_sem=far_recv.at[index],
            device_id=(to, tp),
            device_id_type=MESH,
        )

    def dispatch(step, carry):
        to = lax.rem(ep + step, n_ep)
        far(outgoing.at[to], recv.at[tp, ep], to, 0).start()
        return carry

    lax.fori_loop(1, n_ep, dispatch, 0)
    recv[tp, ep] = outgoing[ep]
    some = pl.ds(0, n_ep - 1)
    all_dispatched = far(outgoing.at[some], recv.at[tp, some], ep, 0)
    all_dispatched.wait_recv()
    forward = to_pair(recv.at[tp], recv.at[tp], 4)
    forward.start()
    for load in loads[5:]:
        load.wait()
    stage[0, :, :cap] = recv[tp].astype(F32)
    own_rows = stage[0].reshape(slots, half).astype(BF16)
    gate_part = dot(own_rows, w_gate[mine])
    up_part = dot(own_rows, w_up[mine])
    forward.wait_recv()
    stage[1, :, :cap] = recv[other].astype(F32)
    peer_rows = stage[1].reshape(slots, half).astype(BF16)
    gate_part = gate_part + dot(peer_rows, w_gate[theirs])
    up_part = up_part + dot(peer_rows, w_up[theirs])
    hid[tp] = (jax.nn.silu(gate_part) * up_part).astype(BF16)
    send_hid = to_pair(hid.at[tp], hid.at[tp], 5)
    send_hid.start()
    result = dot(hid[tp], w_down[tp])
    send_down.wait_recv()
    send_hid.wait_recv()
    result = result + dot(hid[other], w_down[other])
    ret[...] = result.reshape(n_ep, pad, half)[:, :cap].astype(BF16)

    def give_back(step, carry):
        to = lax.rem(ep + step, n_ep)
        far(ret.at[to], back.at[ep], to, 1).start()
        return carry

    lax.fori_loop(1, n_ep, give_back, 0)
    back[ep] = ret[ep]
    all_returned = far(ret.at[some], back.at[some], ep, 1)
    all_returned.wait_recv()
    back_stage[:, :cap] = back[...].astype(F32)
    rows = back_stage[...].reshape(slots, half).astype(BF16)
    total = weights[:, 0:1] * dot(pick_a, rows) + weights[:, 1:2] * dot(pick_b, rows)
    layer_out[...] = (values + total).astype(BF16)

    for copy in (send_tokens, send_down, send_mixed, send_squares, forward, send_hid):
        copy.wait_send()
    all_dispatched.wait_send()
    all_returned.wait_send()


def local(n_ep, *args):
    names = list(args)
    tokens, conv_state, hidden_state = names[:3]
    seq, half = tokens.shape
    chans = hidden_state.shape[1]
    hidden_units = names[15].shape[2]
    cap = 2 * max(1, seq // n_ep)
    pad = -(-cap // 8) * 8
    for at in (3, 9, 11, 13):
        names[at] = names[at].reshape(1, -1)
    vmem = pl.BlockSpec(memory_space=pltpu.VMEM)
    hbm = pl.BlockSpec(memory_space=pl.ANY)
    specs = [vmem] * len(names)
    for at in (4, 5, 10, 15, 16, 17):
        specs[at] = hbm
    return pl.pallas_call(
        functools.partial(kernel, n_ep, cap),
        out_shape=(
            jax.ShapeDtypeStruct((seq, half), BF16),
            jax.ShapeDtypeStruct((seq, chans), F32),
        ),
        in_specs=specs,
        out_specs=(vmem, vmem),
        scratch_shapes=[
            pltpu.VMEM((2, half, chans), BF16),
            pltpu.VMEM((2, half, chans), BF16),
            pltpu.VMEM((2 * chans, half), BF16),
            pltpu.VMEM((2 * half, hidden_units), BF16),
            pltpu.VMEM((2 * half, hidden_units), BF16),
            pltpu.VMEM((2, hidden_units, half), BF16),
            pltpu.VMEM((seq, half), BF16),
            pltpu.VMEM((2, seq, chans), BF16),
            pltpu.VMEM((2, seq, 128), F32),
            pltpu.VMEM((n_ep, cap, half), BF16),
            pltpu.VMEM((2, n_ep, cap, half), BF16),
            pltpu.VMEM((2, n_ep, pad, half), F32),
            pltpu.VMEM((2, n_ep * pad, hidden_units), BF16),
            pltpu.VMEM((n_ep, cap, half), BF16),
            pltpu.VMEM((n_ep, cap, half), BF16),
            pltpu.VMEM((n_ep, pad, half), F32),
            pltpu.SemaphoreType.DMA((8,)),
            pltpu.SemaphoreType.DMA((6,)),
            pltpu.SemaphoreType.DMA((6,)),
            pltpu.SemaphoreType.DMA((2,)),
            pltpu.SemaphoreType.DMA((2,)),
        ],
        compiler_params=pltpu.CompilerParams(
            collective_id=0, has_side_effects=True, vmem_limit_bytes=60 * 1024 * 1024
        ),
    )(*names)


def solution(mesh):
    return jax.shard_map(
        functools.partial(local, mesh.shape["ep"]),
        mesh=mesh,
        in_specs=(
            P("ep", "tp"),
            P("ep", None, "tp"),
            P("ep", "tp"),
            P(),
            P(None, "tp"),
            P(None, "tp"),
            P(None, "tp"),
            P("tp", None, None),
            P("tp", None, None),
            P("tp"),
            P(None, "tp"),
            P(),
            P("ep", None),
            P("ep"),
            P("ep", None),
            P("ep", None, "tp"),
            P("ep", None, "tp"),
            P("ep", "tp", None),
        ),
        out_specs=(P("ep", "tp"), P("ep", "tp")),
        check_vma=False,
    )
```

time: 82 us -> 38.7 us (0.47)
  Pallas kernels: 0 us -> 30.3 us
  blocking collectives: 27.2 us -> 0 us
  waiting for transfers between devices: 15.8 us -> 0 us
  between operations: 14.4 us -> 0.64 us
  matrix products: 10.9 us -> 0 us
  starting transfers between devices: 6.77 us -> 0 us
  local copies, waits for them, and re-layouts: 4.27 us -> 7.53 us
  other arithmetic: 2.18 us -> 0 us
    pallas_call x0 -> x1, Pallas kernels: none -> 30.3 us  [local(): pl.pallas_call(functools.partial(kernel, n_ep, cap), out_shape=(jax.Shape...]
    all_to_all x1 -> x0, blocking collectives: 18.2 us -> none  [local(): lax.all_to_all(outgoing, 'ep', split_axis=0, concat_axis=0, tiled=True)]
    dot_general x9 -> x0, matrix products: 10.9 us -> none  [the longest x1 2.27 us: local(): jnp.dot(hidden_units, expert_down[0], preferred_element_type=jnp.float32)]
    all_to_all x1 -> x0, waiting for transfers between devices: 9.95 us -> none  [local(): lax.all_to_all(summed, 'ep', split_axis=0, concat_axis=0, tiled=True)]
    unnamed x29 -> x5, local copies, waits for them, and re-layouts: 0.17 us -> 7.53 us
    all_to_all x1 -> x0, starting transfers between devices: 6.73 us -> none  [local(): lax.all_to_all(summed, 'ep', split_axis=0, concat_axis=0, tiled=True)]
    all_gather x3 -> x0, blocking collectives: 6.48 us -> none  [the longest x1 2.42 us: local(): whole_tokens = lax.all_gather(tokens, 'tp', axis=1, tiled=True)]
    reduce_scatter x1 -> x0, waiting for transfers between devices: 5.84 us -> none  [local(): lax.psum_scatter(partial_value.astype(jnp.bfloat16), 'tp', scatter_dimens...]
  transfers between devices with their start and end apart: 2 -> 0, of which waited for: 2 -> 0; matrix products, arithmetic and copies ran while one was open for 1% -> 0% of each run, Pallas kernels for 0% -> 0%
where the time goes in v1:
time: 38.7 us; the launch traced here: 38.4 us
  Pallas kernels  30.3 us (78%)
  local copies, waits for them, and re-layouts  7.53 us (19%)
  between operations  0.64 us (2%)
    pallas_call x1, Pallas kernels, local(): pl.pallas_call(functools.partial(kernel, n_ep, cap), out_shape=(jax.Shape...  30.3 us
    unnamed x5, local copies, waits for them, and re-layouts  7.53 us

profile of v1, /device:TPU:0, one launch (start us, length us, event | category | flops | bytes accessed | tf_op | source)
XLA Modules:
  0.0 38.4 jit_solution(9303600601424907715)
XLA Ops:
  0.6 1.4 %copy.21.expert_ids = s32[48,2]{1,0:T(8,128)} copy(s32[48,2]{0,1:T(2,128)} %param.30) | data formatting | bytes 768 | tf_op args[12]
  2.0 1.4 %copy.22.expert_logit = f32[48,2]{1,0:T(8,128)} copy(f32[48,2]{0,1:T(2,128)} %param.32) | data formatting | bytes 768 | tf_op args[14]
  3.4 1.7 %copy.20.conv_state = bf16[48,3,512]{2,1,0:T(4,128)(2,1)} copy(bf16[48,3,512]{2,0,1:T(8,128)(2,1)} %param.19) | data formatting | bytes 294912 | tf_op args[1]
  5.1 30.3 %shard_map.185 = (bf16[48,1024]{1,0:T(8,128)(2,1)}, f32[48,512]{1,0:T(8,128)}) custom-call(bf16[48,1024]{1,0:T(8,128)(2,1)} %tokens.1, bf16[48,3,512]{2,1,0:T(4,128)(2,1)} %copy.20.conv_state, f32[48,512]{1,0:T(8,128)} %hidden_state.1, f32[1,2048]{1,0:T(1,128)} %bitcast.4, bf16[2048,512]{1,0:T(8,128)(2,1)} %branch_weight.1, bf16[2048,512]{1,0:T(8,128)(2,1)} %gelu_weight.1, ...), custom_call_target="tpu_custom_call" | custom-call | tf_op jit(solution)/shard_map/pallas_call | solution.py:304
  35.4 1.5 %copy.25 = bf16[48,1024]{1,0:T(8,128)(2,1)} copy(bf16[48,1024]{1,0:T(8,128)(2,1)} %get-tuple-element.4) | data formatting | bytes 196608
  36.9 1.5 %copy.26 = f32[48,512]{1,0:T(8,128)} copy(f32[48,512]{1,0:T(8,128)} %get-tuple-element.5) | data formatting | bytes 196608

commit v2 on v1

--- a/solution.py
+++ b/solution.py
@@ -9,6 +9,7 @@
 
 EPSILON = 1e-06
 RATE_SCALE = 8.0
+VMEM_BYTES = 67_043_328
 MESH = pl.DeviceIdType.MESH
 F32 = jnp.float32
 BF16 = jnp.bfloat16
@@ -122,9 +123,16 @@
     stage[...] = jnp.zeros_like(stage)
     back_stage[...] = jnp.zeros_like(back_stage)
     eye = iota((seq, seq), 0) == iota((seq, seq), 1)
-    ids = expert_ids[...]
-    first, second = ids[:, 0:1], ids[:, 1:2]
-    lane_e = iota((seq, n_ep), 1)
+
+    def as_row(column):
+        return jnp.sum(jnp.where(eye, column, 0.0), axis=0, keepdims=True)
+
+    def as_column(row):
+        return jnp.sum(jnp.where(eye, row, 0.0), axis=1, keepdims=True)
+
+    ids = expert_ids[...].astype(F32)
+    first, second = as_column(ids[0:1]), as_column(ids[1:2])
+    lane_e = iota((seq, n_ep), 1).astype(F32)
     is_first, is_second = lane_e == first, lane_e == second
     named = jnp.where(is_first | is_second, 1.0, 0.0).astype(BF16)
     before = jnp.where(iota((seq, seq), 1) < iota((seq, seq), 0), 1.0, 0.0).astype(BF16)
@@ -132,12 +140,9 @@
 
     def slot_of(chosen, hits):
         rank = jnp.sum(jnp.where(hits, earlier, 0.0), axis=1, keepdims=True)
-        return chosen.astype(F32) * float(pad) + rank
+        return chosen * float(pad) + rank
 
     slot_a, slot_b = slot_of(first, is_first), slot_of(second, is_second)
-
-    def as_row(column):
-        return jnp.sum(jnp.where(eye, column, 0.0), axis=0, keepdims=True)
 
     lane_s = iota((seq, slots), 1).astype(F32)
     pick_a = jnp.where(lane_s == slot_a, 1.0, 0.0).astype(BF16)
@@ -145,12 +150,12 @@
     row_s = iota((slots, seq), 0).astype(F32)
     placed = (row_s == as_row(slot_a)) | (row_s == as_row(slot_b))
     placing = jnp.where(placed, 1.0, 0.0).astype(BF16)
-    prob = jnp.sum(jnp.where(eye, group_prob[...], 0.0), axis=1, keepdims=True)
     logit_exp = jnp.exp(expert_logit[...])
-    weights = prob * logit_exp / jnp.sum(logit_exp, axis=1, keepdims=True)
+    weights = group_prob[...] * logit_exp / jnp.sum(logit_exp, axis=0, keepdims=True)
+    weight_a, weight_b = as_column(weights[0:1]), as_column(weights[1:2])
 
     taps = conv_kernel[...]
-    stored = jnp.sum(conv_state[...].astype(F32) * taps[None, :3], axis=1)
+    stored = sum(conv_state[j].astype(F32) * taps[j : j + 1] for j in range(3))
 
     blocks, block = recur_blocks.shape[0], recur_blocks.shape[1]
     wide = 2 * block
@@ -277,7 +282,7 @@
     all_returned.wait_recv()
     back_stage[:, :cap] = back[...].astype(F32)
     rows = back_stage[...].reshape(slots, half).astype(BF16)
-    total = weights[:, 0:1] * dot(pick_a, rows) + weights[:, 1:2] * dot(pick_b, rows)
+    total = weight_a * dot(pick_a, rows) + weight_b * dot(pick_b, rows)
     layer_out[...] = (values + total).astype(BF16)
 
     for copy in (send_tokens, send_down, send_mixed, send_squares, forward, send_hid):
@@ -296,16 +301,19 @@
     pad = -(-cap // 8) * 8
     for at in (3, 9, 11, 13):
         names[at] = names[at].reshape(1, -1)
+    names[1] = conv_state.transpose(1, 0, 2)
+    for at in (12, 14):
+        names[at] = names[at].T
     vmem = pl.BlockSpec(memory_space=pltpu.VMEM)
-    hbm = pl.BlockSpec(memory_space=pl.ANY)
+    hbm = pl.BlockSpec(memory_space=pltpu.HBM)
     specs = [vmem] * len(names)
     for at in (4, 5, 10, 15, 16, 17):
         specs[at] = hbm
     return pl.pallas_call(
         functools.partial(kernel, n_ep, cap),
         out_shape=(
-            jax.ShapeDtypeStruct((seq, half), BF16),
-            jax.ShapeDtypeStruct((seq, chans), F32),
+            pltpu.VMEM((seq, half), BF16),
+            pltpu.VMEM((seq, chans), F32),
         ),
         in_specs=specs,
         out_specs=(vmem, vmem),
@@ -333,7 +341,7 @@
             pltpu.SemaphoreType.DMA((2,)),
         ],
         compiler_params=pltpu.CompilerParams(
-            collective_id=0, has_side_effects=True, vmem_limit_bytes=60 * 1024 * 1024
+            collective_id=0, has_side_effects=True, vmem_limit_bytes=VMEM_BYTES - 4 * seq * half
         ),
     )(*names)
 

time: 38.7 us -> 31.6 us (0.82)
  local copies, waits for them, and re-layouts: 7.53 us -> 1.28 us
  Pallas kernels: 30.3 us -> 29.6 us
    unnamed x5 -> x2, local copies, waits for them, and re-layouts: 7.53 us -> 1.28 us
    pallas_call x1, Pallas kernels: 30.3 us -> 29.6 us  [local(): pl.pallas_call(functools.partial(kernel, n_ep, cap), out_shape=(pltpu.VME...]
where the time goes in v2:
time: 31.6 us; the launch traced here: 31.5 us
  Pallas kernels  29.6 us (94%)
  local copies, waits for them, and re-layouts  1.28 us (4%)
  between operations  0.65 us (2%)
    pallas_call x1, Pallas kernels, local(): pl.pallas_call(functools.partial(kernel, n_ep, cap), out_shape=(pltpu.VME...  29.6 us
    unnamed x2, local copies, waits for them, and re-layouts  1.28 us

profile of v2, /device:TPU:0, one launch (start us, length us, event | category | flops | bytes accessed | tf_op | source)
XLA Modules:
  0.0 31.5 jit_solution(13479709307701788787)
XLA Ops:
  0.6 29.6 %shard_map.185 = (bf16[48,1024]{1,0:T(8,128)(2,1)S(1)}, f32[48,512]{1,0:T(8,128)S(1)}) custom-call(bf16[48,1024]{1,0:T(8,128)(2,1)} %tokens.1, bf16[3,48,512]{2,1,0:T(8,128)(2,1)} %bitcast.7, f32[48,512]{1,0:T(8,128)} %hidden_state.1, f32[1,2048]{1,0:T(1,128)} %bitcast.8, bf16[2048,512]{1,0:T(8,128)(2,1)} %branch_weight.1, bf16[2048,512]{1,0:T(8,128)(2,1)} %gelu_weight.1, ...), custom_call_target="tpu_custom_call" | custom-call | tf_op jit(solution)/shard_map/pallas_call | solution.py:312
  30.2 0.6 %copy.22 = bf16[48,1024]{1,0:T(8,128)(2,1)} copy(bf16[48,1024]{1,0:T(8,128)(2,1)S(1)} %get-tuple-element.2) | data formatting | bytes 196608
  30.8 0.6 %copy.23 = f32[48,512]{1,0:T(8,128)} copy(f32[48,512]{1,0:T(8,128)S(1)} %get-tuple-element.3) | data formatting | bytes 196608

commit v3 on v2

--- a/solution.py
+++ b/solution.py
@@ -33,21 +33,21 @@
 def kernel(
     n_ep,
     cap,
-    tokens,
-    conv_state,
-    hidden_state,
-    mixer_gain,
+    tokens_in,
+    conv_state_in,
+    hidden_state_in,
+    mixer_gain_in,
     branch_weight,
     gelu_weight,
-    conv_kernel,
-    recur_blocks,
-    input_blocks,
-    decay_rate,
+    conv_kernel_in,
+    recur_blocks_in,
+    input_blocks_in,
+    decay_rate_in,
     output_weight,
-    expert_gain,
-    expert_ids,
-    group_prob,
-    expert_logit,
+    expert_gain_in,
+    expert_ids_in,
+    group_prob_in,
+    expert_logit_in,
     expert_gate,
     expert_up,
     expert_down,
@@ -61,7 +61,6 @@
     w_down,
     tok,
     mixed,
-    squares,
     outgoing,
     recv,
     stage,
@@ -69,7 +68,20 @@
     ret,
     back,
     back_stage,
+    tokens,
+    conv_state,
+    hidden_state,
+    mixer_gain,
+    conv_kernel,
+    recur_blocks,
+    input_blocks,
+    decay_rate,
+    expert_gain,
+    expert_ids,
+    group_prob,
+    expert_logit,
     load_sem,
+    small_sem,
     pair_send,
     pair_recv,
     far_send,
@@ -83,6 +95,56 @@
     pad = stage.shape[2]
     slots = n_ep * pad
 
+    def partner(step):
+        if n_ep & (n_ep - 1):
+            return lax.rem(ep + step, n_ep)
+        to, weight = 0, 1
+        while weight < n_ep:
+            bit = ep // weight % 2 + step // weight % 2
+            to = to + bit % 2 * weight
+            weight *= 2
+        return to
+
+    def each_partner(act):
+        if n_ep <= 16:
+            for step in range(n_ep - 1, 0, -1):
+                act(partner(step))
+        else:
+
+            def body(index, carry):
+                act(partner(n_ep - 1 - index))
+                return carry
+
+            lax.fori_loop(0, n_ep - 1, body, 0)
+
+    barrier = pltpu.get_barrier_semaphore()
+
+    def greet(to):
+        pl.semaphore_signal(barrier, inc=1, device_id=(to, tp), device_id_type=MESH)
+
+    each_partner(greet)
+    pl.semaphore_signal(barrier, inc=1, device_id=(ep, other), device_id_type=MESH)
+
+    small_pairs = (
+        (tokens_in, tokens),
+        (conv_state_in, conv_state),
+        (hidden_state_in, hidden_state),
+        (mixer_gain_in, mixer_gain),
+        (conv_kernel_in, conv_kernel),
+        (recur_blocks_in, recur_blocks),
+        (input_blocks_in, input_blocks),
+        (decay_rate_in, decay_rate),
+        (expert_gain_in, expert_gain),
+        (expert_ids_in, expert_ids),
+        (group_prob_in, group_prob),
+        (expert_logit_in, expert_logit),
+    )
+    smalls = [
+        pltpu.make_async_copy(src, dst, small_sem.at[at])
+        for at, (src, dst) in enumerate(small_pairs)
+    ]
+    for load in smalls:
+        load.start()
     mine = pl.ds(pl.multiple_of(tp * half, half), half)
     theirs = pl.ds(pl.multiple_of(other * half, half), half)
 
@@ -96,19 +158,6 @@
         pltpu.make_async_copy(expert_up.at[0], w_up, load_sem.at[6]),
         pltpu.make_async_copy(expert_down.at[0, :, mine], w_down.at[tp], load_sem.at[7]),
     ]
-    for load in loads:
-        load.start()
-
-    barrier = pltpu.get_barrier_semaphore()
-    pl.semaphore_signal(barrier, inc=1, device_id=(ep, other), device_id_type=MESH)
-
-    def greet(step, carry):
-        pl.semaphore_signal(
-            barrier, inc=1, device_id=(lax.rem(ep + step, n_ep), tp), device_id_type=MESH
-        )
-        return carry
-
-    lax.fori_loop(1, n_ep, greet, 0)
 
     def to_pair(src, dst, index):
         return pltpu.make_async_remote_copy(
@@ -122,6 +171,10 @@
 
     stage[...] = jnp.zeros_like(stage)
     back_stage[...] = jnp.zeros_like(back_stage)
+    for load in smalls:
+        load.wait()
+    for load in loads:
+        load.start()
     eye = iota((seq, seq), 0) == iota((seq, seq), 1)
 
     def as_row(column):
@@ -217,16 +270,7 @@
     residual = (residual + dot(mixed[other], w_out[their_rows])).astype(BF16)
 
     values = residual.astype(F32)
-    mine_square = jnp.sum(values * values, axis=1, keepdims=True)
-    squares[tp] = jnp.broadcast_to(mine_square, squares.shape[1:])
-    send_squares = to_pair(squares.at[tp], squares.at[tp], 3)
-    send_squares.start()
-    chosen = dot(placing, residual) * expert_gain[:, mine]
-    send_squares.wait_recv()
-    both = mine_square + squares[other][:, 0:1]
-    scaling = as_row(lax.rsqrt(both / (2 * half) + EPSILON))
-    slot_scale = jnp.sum(jnp.where(placed, scaling, 0.0), axis=1, keepdims=True)
-    chosen = (chosen * slot_scale).reshape(n_ep, pad, half)
+    chosen = dot(placing, residual).reshape(n_ep, pad, half)
     outgoing[...] = chosen[:, :cap].astype(BF16)
 
     def far(src, dst, to, index):
@@ -239,31 +283,31 @@
             device_id_type=MESH,
         )
 
-    def dispatch(step, carry):
-        to = lax.rem(ep + step, n_ep)
-        far(outgoing.at[to], recv.at[tp, ep], to, 0).start()
-        return carry
-
-    lax.fori_loop(1, n_ep, dispatch, 0)
+    each_partner(lambda to: far(outgoing.at[to], recv.at[tp, ep], to, 0).start())
     recv[tp, ep] = outgoing[ep]
     some = pl.ds(0, n_ep - 1)
     all_dispatched = far(outgoing.at[some], recv.at[tp, some], ep, 0)
     all_dispatched.wait_recv()
-    forward = to_pair(recv.at[tp], recv.at[tp], 4)
+    forward = to_pair(recv.at[tp], recv.at[tp], 3)
     forward.start()
     for load in loads[5:]:
         load.wait()
     stage[0, :, :cap] = recv[tp].astype(F32)
-    own_rows = stage[0].reshape(slots, half).astype(BF16)
+    raw = stage[0].reshape(slots, half)
+    row_square = jnp.sum(raw * raw, axis=1, keepdims=True)
+    own_rows = (raw * expert_gain[:, mine]).astype(BF16)
     gate_part = dot(own_rows, w_gate[mine])
     up_part = dot(own_rows, w_up[mine])
     forward.wait_recv()
     stage[1, :, :cap] = recv[other].astype(F32)
-    peer_rows = stage[1].reshape(slots, half).astype(BF16)
-    gate_part = gate_part + dot(peer_rows, w_gate[theirs])
-    up_part = up_part + dot(peer_rows, w_up[theirs])
+    raw = stage[1].reshape(slots, half)
+    row_square = row_square + jnp.sum(raw * raw, axis=1, keepdims=True)
+    row_scale = lax.rsqrt(row_square / (2 * half) + EPSILON)
+    peer_rows = (raw * expert_gain[:, theirs]).astype(BF16)
+    gate_part = (gate_part + dot(peer_rows, w_gate[theirs])) * row_scale
+    up_part = (up_part + dot(peer_rows, w_up[theirs])) * row_scale
     hid[tp] = (jax.nn.silu(gate_part) * up_part).astype(BF16)
-    send_hid = to_pair(hid.at[tp], hid.at[tp], 5)
+    send_hid = to_pair(hid.at[tp], hid.at[tp], 4)
     send_hid.start()
     result = dot(hid[tp], w_down[tp])
     send_down.wait_recv()
@@ -271,12 +315,7 @@
     result = result + dot(hid[other], w_down[other])
     ret[...] = result.reshape(n_ep, pad, half)[:, :cap].astype(BF16)
 
-    def give_back(step, carry):
-        to = lax.rem(ep + step, n_ep)
-        far(ret.at[to], back.at[ep], to, 1).start()
-        return carry
-
-    lax.fori_loop(1, n_ep, give_back, 0)
+    each_partner(lambda to: far(ret.at[to], back.at[ep], to, 1).start())
     back[ep] = ret[ep]
     all_returned = far(ret.at[some], back.at[some], ep, 1)
     all_returned.wait_recv()
@@ -285,10 +324,21 @@
     total = weight_a * dot(pick_a, rows) + weight_b * dot(pick_b, rows)
     layer_out[...] = (values + total).astype(BF16)
 
-    for copy in (send_tokens, send_down, send_mixed, send_squares, forward, send_hid):
+    for copy in (send_tokens, send_down, send_mixed, forward, send_hid):
         copy.wait_send()
     all_dispatched.wait_send()
     all_returned.wait_send()
+
+
+def write_out(rows, hidden, rows_out, hidden_out, sems):
+    copies = [
+        pltpu.make_async_copy(rows, rows_out, sems.at[0]),
+        pltpu.make_async_copy(hidden, hidden_out, sems.at[1]),
+    ]
+    for copy in copies:
+        copy.start()
+    for copy in copies:
+        copy.wait()
 
 
 def local(n_ep, *args):
@@ -306,16 +356,14 @@
         names[at] = names[at].T
     vmem = pl.BlockSpec(memory_space=pltpu.VMEM)
     hbm = pl.BlockSpec(memory_space=pltpu.HBM)
-    specs = [vmem] * len(names)
-    for at in (4, 5, 10, 15, 16, 17):
-        specs[at] = hbm
-    return pl.pallas_call(
+    small = (0, 1, 2, 3, 6, 7, 8, 9, 11, 12, 13, 14)
+    results = pl.pallas_call(
         functools.partial(kernel, n_ep, cap),
         out_shape=(
             pltpu.VMEM((seq, half), BF16),
             pltpu.VMEM((seq, chans), F32),
         ),
-        in_specs=specs,
+        in_specs=[hbm] * len(names),
         out_specs=(vmem, vmem),
         scratch_shapes=[
             pltpu.VMEM((2, half, chans), BF16),
@@ -326,7 +374,6 @@
             pltpu.VMEM((2, hidden_units, half), BF16),
             pltpu.VMEM((seq, half), BF16),
             pltpu.VMEM((2, seq, chans), BF16),
-            pltpu.VMEM((2, seq, 128), F32),
             pltpu.VMEM((n_ep, cap, half), BF16),
             pltpu.VMEM((2, n_ep, cap, half), BF16),
             pltpu.VMEM((2, n_ep, pad, half), F32),
@@ -334,9 +381,11 @@
             pltpu.VMEM((n_ep, cap, half), BF16),
             pltpu.VMEM((n_ep, cap, half), BF16),
             pltpu.VMEM((n_ep, pad, half), F32),
+            *[pltpu.VMEM(names[at].shape, names[at].dtype) for at in small],
             pltpu.SemaphoreType.DMA((8,)),
-            pltpu.SemaphoreType.DMA((6,)),
-            pltpu.SemaphoreType.DMA((6,)),
+            pltpu.SemaphoreType.DMA((len(small),)),
+            pltpu.SemaphoreType.DMA((5,)),
+            pltpu.SemaphoreType.DMA((5,)),
             pltpu.SemaphoreType.DMA((2,)),
             pltpu.SemaphoreType.DMA((2,)),
         ],
@@ -344,6 +393,17 @@
             collective_id=0, has_side_effects=True, vmem_limit_bytes=VMEM_BYTES - 4 * seq * half
         ),
     )(*names)
+    return pl.pallas_call(
+        write_out,
+        out_shape=(
+            jax.ShapeDtypeStruct((seq, half), BF16),
+            jax.ShapeDtypeStruct((seq, chans), F32),
+        ),
+        in_specs=[pl.BlockSpec(memory_space=pltpu.VMEM)] * 2,
+        out_specs=(hbm, hbm),
+        scratch_shapes=[pltpu.SemaphoreType.DMA((2,))],
+        compiler_params=pltpu.CompilerParams(vmem_limit_bytes=1 << 20),
+    )(*results)
 
 
 def solution(mesh):

time: 31.6 us -> 29.6 us (0.937)
  local copies, waits for them, and re-layouts: 1.28 us -> 0 us
  Pallas kernels: 29.6 us -> 28.8 us
    pallas_call x1, Pallas kernels: 29.6 us -> 28.2 us  [local(): pl.pallas_call(functools.partial(kernel, n_ep, cap), out_shape=(pltpu.VME...]
    unnamed x2 -> x0, local copies, waits for them, and re-layouts: 1.28 us -> none
    pallas_call x0 -> x1, Pallas kernels: none -> 0.69 us  [local(): pl.pallas_call(write_out, out_shape=(jax.ShapeDtypeStruct((seq, half), BF...]
where the time goes in v3:
time: 29.6 us; the launch traced here: 29.5 us
  Pallas kernels  28.8 us (97%)
  between operations  0.65 us (2%)
    pallas_call x1, Pallas kernels, local(): pl.pallas_call(functools.partial(kernel, n_ep, cap), out_shape=(pltpu.VME...  28.2 us
    pallas_call x1, Pallas kernels, local(): pl.pallas_call(write_out, out_shape=(jax.ShapeDtypeStruct((seq, half), BF...  0.69 us

profile of v3, /device:TPU:0, one launch (start us, length us, event | category | flops | bytes accessed | tf_op | source)
XLA Modules:
  0.0 29.5 jit_solution(8572298963547762078)
XLA Ops:
  0.6 28.2 %shard_map.185 = (bf16[48,1024]{1,0:T(8,128)(2,1)S(1)}, f32[48,512]{1,0:T(8,128)S(1)}) custom-call(bf16[48,1024]{1,0:T(8,128)(2,1)} %tokens_in.1, bf16[3,48,512]{2,1,0:T(8,128)(2,1)} %bitcast.7, f32[48,512]{1,0:T(8,128)} %hidden_state_in.1, f32[1,2048]{1,0:T(1,128)} %bitcast.8, bf16[2048,512]{1,0:T(8,128)(2,1)} %branch_weight.1, ...), custom_call_target="tpu_custom_call" | custom-call | tf_op jit(solution)/shard_map/pallas_call | solution.py:360
  28.8 0.7 %shard_map.186 = (bf16[48,1024]{1,0:T(8,128)(2,1)}, f32[48,512]{1,0:T(8,128)}) custom-call(bf16[48,1024]{1,0:T(8,128)(2,1)S(1)} %get-tuple-element.4.rows, f32[48,512]{1,0:T(8,128)S(1)} %get-tuple-element.5.hidden), custom_call_target="tpu_custom_call" | custom-call | tf_op jit(solution)/shard_map/pallas_call | solution.py:396
